TPU v7x, 32 devices: a whole 2x2x4 slice. The times are simulated.
32 devices in a mesh: st: 8 (over z, y), tp: 4 (over x, core).
Axes of the slice: x: 2, y: 2, z: 4, core: 2. Of those that a mesh axis runs over, the one named last changes fastest.
Arguments:
- queries: bfloat16 [8192, 1024], P('st', 'tp'), may hold values from -540 to 540
- gate_pre: bfloat16 [8192, 1024], P('st', 'tp'), may hold values from -6 to 6
- cotangent: bfloat16 [8192, 1024], P('st', 'tp'), may hold values from -6 to 6
- store: bfloat16 [10240, 2048], P('st'), may hold values from -6 to 6
- store_gain: float32 [2048], replicated, may hold values from 0.1 to 1.9
- w_key: bfloat16 [2048, 1024], P(None, 'tp'), may hold values from -0.125 to 0.125
- w_value: bfloat16 [2048, 1024], P(None, 'tp'), may hold values from -0.125 to 0.125
- owners: int32 [64, 4], P('st'), may hold values from 0 to 7, all different within a row; in each aligned block of 8 rows (0 to 7, 8 to 15, ...) at most 8 rows name the same one
- slots: int32 [64, 4], P('st'), may hold values from 0 to 19
Outputs:
- grad_queries: float32 [8192, 1024], P('st', 'tp')
- grad_store: float32 [10240, 2048], P(('st', 'tp'))
- grad_w_value: float32 [2048, 1024], P('st', 'tp')
Inputs may be any that keep to these rules, and one draw needn't show every extreme that they name: Each block names 4 different owners. Among the blocks of one device no owner is named twice.
All inputs are finite; a program needn't handle non-finite values.
Results may differ from a plain program's by a relative error of at most 0.014.
Values may be sent and summed in bfloat16 or wider, within the bound.
A program may use at most 192 MiB of HBM per device.

v0:
```python
import jax
import jax.numpy as jnp
from jax import lax
from jax.sharding import PartitionSpec as P

HD = 128
PLEN = 64


EPS = 1e-06


def row_scale(store_rows):
    return lax.rsqrt(jnp.mean(store_rows * store_rows, axis=-1, keepdims=True) + EPS)


def contract(left, right):
    return lax.dot_general(
        left, right, (((1,), (1,)), ((), ())), preferred_element_type=jnp.float32
    )


def local(queries, gate_pre, cotangent, store, store_gain, w_key, w_value, owners, slots):
    st_size = lax.axis_size("st")
    tp_size = lax.axis_size("tp")
    blocks, per_block = owners.shape
    tok_rows, local_width = queries.shape
    head_dim = HD
    local_heads = local_width // head_dim
    block_len = tok_rows // blocks
    passage_len = PLEN
    rows_dev = store.shape[0]
    passages = rows_dev // passage_len
    slot_count = blocks * per_block
    slot_cap = (2 * slot_count + st_size - 1) // st_size
    store_rows = store.astype(jnp.float32)
    row_inverse = row_scale(store_rows)
    normed = (store_rows * row_inverse * store_gain).astype(jnp.bfloat16)
    key_table = jnp.dot(normed, w_key, preferred_element_type=jnp.float32).astype(jnp.bfloat16)
    value_table = jnp.dot(normed, w_value, preferred_element_type=jnp.float32).astype(jnp.bfloat16)
    key_table = key_table.reshape(passages, passage_len, local_width)
    value_table = value_table.reshape(passages, passage_len, local_width)
    owner_flat = owners.reshape(slot_count)
    slot_flat = slots.reshape(slot_count)
    slot_order = jnp.arange(slot_count, dtype=jnp.int32)
    earlier_same = (owner_flat[:, None] == owner_flat[None, :]) & (
        slot_order[None, :] < slot_order[:, None]
    )
    slot_rank = jnp.sum(earlier_same.astype(jnp.int32), axis=1)
    position = owner_flat * slot_cap + slot_rank
    places = jnp.arange(st_size * slot_cap, dtype=jnp.int32)
    slot_hits = position[:, None] == places[None, :]
    requests = jnp.sum(jnp.where(slot_hits, slot_flat[:, None], 0), axis=0)
    requests = requests.reshape(st_size, slot_cap)
    asked_ids = lax.all_to_all(requests, "st", split_axis=0, concat_axis=0, tiled=True)
    asked_flat = asked_ids.reshape(-1)
    shape_out = asked_ids.shape + (passage_len, local_width)
    picked_keys = jnp.take(key_table, asked_flat, axis=0).reshape(shape_out)
    picked_values = jnp.take(value_table, asked_flat, axis=0).reshape(shape_out)
    sent_keys = lax.all_to_all(picked_keys, "st", split_axis=0, concat_axis=0, tiled=True)
    sent_values = lax.all_to_all(picked_values, "st", split_axis=0, concat_axis=0, tiled=True)
    got_keys, got_values, asked_ids = (sent_keys, sent_values, asked_ids)
    span = per_block * passage_len
    mine_keys = jnp.take(
        got_keys.reshape(st_size * slot_cap, passage_len, local_width), position, axis=0
    )
    mine_values = jnp.take(
        got_values.reshape(st_size * slot_cap, passage_len, local_width), position, axis=0
    )
    mine_keys = mine_keys.reshape(blocks, span, local_heads, head_dim)
    mine_values = mine_values.reshape(blocks, span, local_heads, head_dim)
    score_scale = head_dim ** (-0.5)
    query_blocks = queries.reshape(blocks, block_len, local_heads, head_dim)
    gate_open = jax.nn.sigmoid(gate_pre.astype(jnp.float32))
    grad_in = (gate_open * cotangent.astype(jnp.float32)).astype(jnp.bfloat16)
    grad_in = grad_in.reshape(blocks, block_len, local_heads, head_dim)
    scores = (
        jnp.einsum("bqhd,bkhd->bhqk", query_blocks, mine_keys, preferred_element_type=jnp.float32)
        * score_scale
    )
    shifted = scores - jnp.max(scores, axis=-1, keepdims=True)
    weights = jnp.exp(shifted)
    weights = weights / jnp.sum(weights, axis=-1, keepdims=True)
    weights_half = weights.astype(jnp.bfloat16)
    attended = jnp.einsum(
        "bhqk,bkhd->bqhd", weights_half, mine_values, preferred_element_type=jnp.float32
    )
    row_delta = jnp.sum(grad_in.astype(jnp.float32) * attended, axis=-1)
    grad_weights = jnp.einsum(
        "bqhd,bkhd->bhqk", grad_in, mine_values, preferred_element_type=jnp.float32
    )
    grad_scores = weights * (grad_weights - jnp.transpose(row_delta, (0, 2, 1))[..., None])
    grad_half = grad_scores.astype(jnp.bfloat16)
    grad_queries = (
        jnp.einsum("bhqk,bkhd->bqhd", grad_half, mine_keys, preferred_element_type=jnp.float32)
        * score_scale
    )
    grad_queries = grad_queries.reshape(tok_rows, local_width)
    grad_keys = (
        jnp.einsum("bhqk,bqhd->bkhd", grad_half, query_blocks, preferred_element_type=jnp.float32)
        * score_scale
    )
    grad_values = jnp.einsum(
        "bhqk,bqhd->bkhd", weights_half, grad_in, preferred_element_type=jnp.float32
    )
    grad_keys = grad_keys.reshape(slot_count, passage_len, local_width)
    grad_values = grad_values.reshape(slot_count, passage_len, local_width)
    empty_slots = jnp.zeros((st_size * slot_cap, passage_len, local_width), jnp.float32)
    outgoing_keys = empty_slots.at[position].set(grad_keys)
    outgoing_values = empty_slots.at[position].set(grad_values)
    back_keys, back_values = (
        lax.all_to_all(outgoing_keys, "st", split_axis=0, concat_axis=0, tiled=True),
        lax.all_to_all(outgoing_values, "st", split_axis=0, concat_axis=0, tiled=True),
    )
    asked_flat = asked_ids.reshape(-1)
    owner_pick = (asked_flat[None, :] == jnp.arange(passages, dtype=jnp.int32)[:, None]).astype(
        jnp.float32
    )
    passage_keys = jnp.dot(
        owner_pick,
        back_keys.reshape(st_size * slot_cap, passage_len * local_width),
        precision=lax.Precision.HIGHEST,
        preferred_element_type=jnp.float32,
    )
    passage_values = jnp.dot(
        owner_pick,
        back_values.reshape(st_size * slot_cap, passage_len * local_width),
        precision=lax.Precision.HIGHEST,
        preferred_element_type=jnp.float32,
    )
    passage_keys = passage_keys.astype(jnp.bfloat16).reshape(rows_dev, local_width)
    passage_values = passage_values.astype(jnp.bfloat16).reshape(rows_dev, local_width)
    weight_terms = lax.dot_general(
        normed, passage_values, (((0,), (0,)), ((), ())), preferred_element_type=jnp.float32
    )
    grad_w_value = lax.psum_scatter(weight_terms, "st", scatter_dimension=0, tiled=True)
    quarter = rows_dev // tp_size
    whole_key, whole_value = (
        lax.all_gather(w_key, "tp", axis=1, tiled=True),
        lax.all_gather(w_value, "tp", axis=1, tiled=True),
    )
    own_keys, own_values = (
        lax.all_to_all(passage_keys, "tp", split_axis=0, concat_axis=1, tiled=True),
        lax.all_to_all(passage_values, "tp", split_axis=0, concat_axis=1, tiled=True),
    )
    grad_normed = contract(own_keys, whole_key) + contract(own_values, whole_value)
    first_row = lax.axis_index("tp") * quarter
    own_rows = lax.dynamic_slice_in_dim(store_rows, first_row, quarter, 0)
    own_inverse = lax.dynamic_slice_in_dim(row_inverse, first_row, quarter, 0)
    unit_rows = own_rows * own_inverse
    grad_unit = grad_normed * store_gain
    grad_store = own_inverse * (
        grad_unit - unit_rows * jnp.mean(grad_unit * unit_rows, axis=-1, keepdims=True)
    )
    return (grad_queries, grad_store, grad_w_value)


def solution(mesh):
    placed = (
        P("st", "tp"),
        P("st", "tp"),
        P("st", "tp"),
        P("st", None),
        P(),
        P(None, "tp"),
        P(None, "tp"),
        P("st", None),
        P("st", None),
    )
    return jax.shard_map(
        local,
        mesh=mesh,
        in_specs=placed,
        out_specs=(P("st", "tp"), P(("st", "tp"), None), P("st", "tp")),
        check_vma=False,
    )
```

profile of v0, /device:TPU:0, one launch (start us, length us, event | category | flops | bytes accessed | tf_op | source)
XLA Modules:
  0.0 424.0 jit_solution(17459146914294661466)
XLA Ops:
  8.0 0.8 copy.71
  9.0 0.8 copy.72
  10.7 7.3 %all-to-all-start = ((s32[8,1,8]{2,1,0:T(1,128)}), s32[8,1,8]{2,1,0:T(1,128)S(1)}, u32[]{:S(2)}, u32[]{:S(2)}) async-start(s32[8,1,8]{2,1,0:T(1,128)} %bitcast), calls=%async_computation | async-start | bytes 8192 | tf_op jit(solution)/shard_map/all_to_all | solution.py:55
  18.0 3.7 multiply_reduce_fusion
  22.0 3.0 convolution_convert_fusion.3
  25.0 1.7 convolution_convert_fusion.2
  28.8 2.0 gather_fusion.2
  30.8 3.3 broadcast_select_fusion
  34.1 53.7 %all_to_all.67 = bf16[8,8,64,256]{3,2,1,0:T(8,128)(2,1)} all-to-all(bf16[8,8,64,256]{3,2,1,0:T(8,128)(2,1)S(1)} %bitcast.71), channel_id=1, replica_groups=mesh['st'=8,'tp'=4] {'st'}, dimensions={0} | all-to-all | bytes 4194304 | tf_op jit(solution)/shard_map/all_to_all | solution.py:60
  87.8 4.5 %all-to-all-start.2 = ((bf16[8,8,64,256]{3,2,1,0:T(8,128)(2,1)}), bf16[8,8,64,256]{3,2,1,0:T(8,128)(2,1)}, u32[]{:S(2)}, u32[]{:S(2)}) async-start(bf16[8,8,64,256]{3,2,1,0:T(8,128)(2,1)} %bitcast.6), calls=%async_computation.2 | async-start | bytes 4194304 | tf_op jit(solution)/shard_map/all_to_all | solution.py:61
  93.6 1.1 copy.79
  94.9 2.2 gather_fusion.1
  97.1 42.4 %all-to-all-done.2 = bf16[8,8,64,256]{3,2,1,0:T(8,128)(2,1)} async-done(((bf16[8,8,64,256]{3,2,1,0:T(8,128)(2,1)}), bf16[8,8,64,256]{3,2,1,0:T(8,128)(2,1)}, u32[]{:S(2)}, u32[]{:S(2)}) %all-to-all-start.2) | async-done | bytes 2097184 | tf_op jit(solution)/shard_map/all_to_all | solution.py:61
  139.5 2.2 gather_fusion.3
  141.7 1.6 broadcast_select_fusion.2
  143.3 1.3 reshape.158
  145.8 1.6 fusion.23
  147.5 1.3 copy-done.8
  149.3 2.3 copy.92
  151.6 2.9 reshape.215
  154.5 2.5 broadcast_in_dim.52.clone.1
  157.0 5.4 %scatter_fusion.1 = f32[64,64,256]{2,1,0:T(8,128)} fusion(f32[64,64,256]{2,1,0:T(8,128)} %broadcast_in_dim.52.clone.1, s32[32]{0:T(128)S(1)} %fusion.18, f32[32,64,256]{2,1,0:T(8,128)S(1)} %reshape.215), kind=kCustom, calls=%fused_computation.5 | custom fusion | bytes 6291584 | tf_op jit(solution)/shard_map/scatter | solution.py:110
  162.4 4.7 %all-to-all-start.5 = ((f32[64,64,256]{2,1,0:T(8,128)}), f32[64,64,256]{2,1,0:T(8,128)}, u32[]{:S(2)}, u32[]{:S(2)}) async-start(f32[64,64,256]{2,1,0:T(8,128)} %scatter_fusion.1), calls=%async_computation.5 | async-start | bytes 8388608 | tf_op jit(solution)/shard_map/all_to_all | solution.py:113
  168.9 2.3 fusion.9
  172.0 1.0 copy-done.3
  173.3 2.9 copy.88
  176.3 3.0 reshape.207
  179.3 2.5 broadcast_in_dim.52.clone
  181.8 5.5 %scatter_fusion = f32[64,64,256]{2,1,0:T(8,128)} fusion(f32[64,64,256]{2,1,0:T(8,128)} %broadcast_in_dim.52.clone, s32[32]{0:T(128)S(1)} %fusion.18, f32[32,64,256]{2,1,0:T(8,128)S(1)} %reshape.207), kind=kCustom, calls=%fused_computation.4 | custom fusion | bytes 6291584 | tf_op jit(solution)/shard_map/scatter | solution.py:109
  187.3 72.3 %all-to-all-done.5 = f32[64,64,256]{2,1,0:T(8,128)} async-done(((f32[64,64,256]{2,1,0:T(8,128)}), f32[64,64,256]{2,1,0:T(8,128)}, u32[]{:S(2)}, u32[]{:S(2)}) %all-to-all-start.5) | async-done | bytes 4194336 | tf_op jit(solution)/shard_map/all_to_all | solution.py:113
  259.6 4.5 %all-to-all-start.3 = ((f32[64,64,256]{2,1,0:T(8,128)}), f32[64,64,256]{2,1,0:T(8,128)}, u32[]{:S(2)}, u32[]{:S(2)}) async-start(f32[64,64,256]{2,1,0:T(8,128)} %scatter_fusion), calls=%async_computation.3 | async-start | bytes 8388608 | tf_op jit(solution)/shard_map/all_to_all | solution.py:112
  264.2 4.6 %copy.109 = f32[8,8,64,256]{3,1,2,0:T(8,128)S(1)} copy(f32[8,8,64,256]{3,2,1,0:T(8,128)} %bitcast.26) | data formatting | bytes 8388608
  268.8 1.5 convolution_convert_fusion
  270.8 5.8 %fusion.22 = f32[2048,256]{1,0:T(8,128)} fusion(bf16[1280,256]{1,0:T(8,128)(2,1)S(1)} %reshape.170, f32[2048]{0:T(1024)S(1)} %copy-done.16, f32[1280]{0:T(1024)S(1)} %add_rsqrt_fusion, bf16[1280,2048]{1,0:T(8,128)(2,1)} %param.16), kind=kOutput, calls=%fused_computation.65 | convolution fusion | flops 1352663040 | bytes 8008704 | tf_op jit(solution)/shard_map/dot_general | solution.py:133
  276.7 1.3 all_to_all.56
  278.0 95.6 %all-to-all-done.3 = f32[64,64,256]{2,1,0:T(8,128)} async-done(((f32[64,64,256]{2,1,0:T(8,128)}), f32[64,64,256]{2,1,0:T(8,128)}, u32[]{:S(2)}, u32[]{:S(2)}) %all-to-all-start.3) | async-done | bytes 4194336 | tf_op jit(solution)/shard_map/all_to_all | solution.py:112
  373.6 3.5 all-to-all-start.6
  377.1 4.6 %copy.108 = f32[8,8,64,256]{3,1,2,0:T(8,128)S(1)} copy(f32[8,8,64,256]{3,2,1,0:T(8,128)} %bitcast.24) | data formatting | bytes 8388608
  381.6 1.5 convolution_convert_fusion.1
  383.2 1.3 all_to_all.51
  384.5 2.8 all-to-all-done.6
  387.3 4.4 %all-to-all-start.4 = ((bf16[4,320,256]{2,1,0:T(8,128)(2,1)}), bf16[4,320,256]{2,1,0:T(8,128)(2,1)}, u32[]{:S(2)}, u32[]{:S(2)}) async-start(bf16[4,320,256]{2,1,0:T(8,128)(2,1)} %all_to_all.51), calls=%async_computation.4 | async-start | bytes 1310720 | tf_op jit(solution)/shard_map/all_to_all | solution.py:143
  391.7 8.1 %convert_element_type.40 = f32[1280,2048]{1,0:T(8,128)} convert(bf16[1280,2048]{1,0:T(8,128)(2,1)} %param.16) | non-fusion elementwise | flops 2621440 | bytes 15728640 | tf_op jit(solution)/shard_map/convert_element_type | solution.py:36
  400.9 1.0 copy.115
  402.0 2.0 copy.105
  404.0 3.9 fusion.24
  408.0 4.9 %multiply_reduce_fusion.1 = (f32[320]{0:T(512)S(1)}, f32[320,2048]{1,0:T(8,128)S(1)}) fusion(f32[1280,2048]{1,0:T(8,128)} %convert_element_type.40, s32[]{:T(128)S(6)} %select_n.34, f32[320]{0:T(512)S(1)} %dynamic-slice.3, f32[2048]{0:T(1024)S(1)} %copy-done.16, f32[320,2048]{1,0:T(8,128)S(1)} %fusion.24, bf16[320,1024]{1,0:T(8,128)(2,1)S(1)} %bitcast.75, ...), kind=kOutput, calls=%fused_computation.14 | convolution fusion | flops 1345453824 | bytes 12724740 | tf_op jit(solution)/shard_map/dot_general | solution.py:18
  412.9 3.7 subtract_multiply_fusion
  (81 shorter events, 11.2 us)
Async XLA Ops:
  10.7 16.1 %all-to-all-start = ((s32[8,1,8]{2,1,0:T(1,128)}), s32[8,1,8]{2,1,0:T(1,128)S(1)}, u32[]{:S(2)}, u32[]{:S(2)}) async-start(s32[8,1,8]{2,1,0:T(1,128)} %bitcast), calls=%async_computation | async-start | bytes 8192 | tf_op jit(solution)/shard_map/all_to_all | solution.py:55
  18.0 4.0 copy-start
  18.0 4.0 copy-start.16
  22.0 3.0 copy-start.10
  87.8 5.2 %copy-start.13 = (bf16[1024,256]{1,0:T(8,128)(2,1)S(1)}, bf16[1024,256]{1,0:T(8,128)(2,1)}, u32[]{:S(2)}) copy-start(bf16[1024,256]{1,0:T(8,128)(2,1)} %param.13) | copy-start | bytes 1572868
  87.8 5.4 %copy-start.11 = (bf16[1024,256]{1,0:T(8,128)(2,1)S(1)}, bf16[1024,256]{1,0:T(8,128)(2,1)}, u32[]{:S(2)}) copy-start(bf16[1024,256]{1,0:T(8,128)(2,1)} %param.15) | copy-start | bytes 1572868
  87.8 5.4 %copy-start.12 = (bf16[1024,256]{1,0:T(8,128)(2,1)S(1)}, bf16[1024,256]{1,0:T(8,128)(2,1)}, u32[]{:S(2)}) copy-start(bf16[1024,256]{1,0:T(8,128)(2,1)} %param.14) | copy-start | bytes 1572868
  87.8 51.7 %all-to-all-start.2 = ((bf16[8,8,64,256]{3,2,1,0:T(8,128)(2,1)}), bf16[8,8,64,256]{3,2,1,0:T(8,128)(2,1)}, u32[]{:S(2)}, u32[]{:S(2)}) async-start(bf16[8,8,64,256]{3,2,1,0:T(8,128)(2,1)} %bitcast.6), calls=%async_computation.2 | async-start | bytes 4194304 | tf_op jit(solution)/shard_map/all_to_all | solution.py:61
  92.3 311.8 %all-gather.3.cloned.1.call-start = ((), (), s32[]{:S(2)}) async-start(), calls=%async_computation.8 | async-start | bytes 5242880 | tf_op jit(solution)/shard_map/all_gather | solution.py:139
  93.0 1.7 copy-start.17
  93.2 52.2 %copy-start.1 = (bf16[8,128,2,128]{3,2,1,0:T(2,128)(2,1)}, bf16[8,128,2,128]{3,2,1,0:T(2,128)(2,1)S(1)}, u32[]{:S(2)}) copy-start(bf16[8,128,2,128]{3,2,1,0:T(2,128)(2,1)S(1)} %reshape.159) | copy-start | bytes 1572868
  145.8 3.0 copy-start.14
  147.5 1.3 copy-start.8
  162.4 5.4 %copy-start.5 = (bf16[32,64,256]{2,1,0:T(8,128)(2,1)S(1)}, bf16[32,64,256]{2,1,0:T(8,128)(2,1)}, u32[]{:S(2)}) copy-start(bf16[32,64,256]{2,1,0:T(8,128)(2,1)} %get-tuple-element.16) | copy-start | bytes 3145732
  162.4 97.2 %all-to-all-start.5 = ((f32[64,64,256]{2,1,0:T(8,128)}), f32[64,64,256]{2,1,0:T(8,128)}, u32[]{:S(2)}, u32[]{:S(2)}) async-start(f32[64,64,256]{2,1,0:T(8,128)} %scatter_fusion.1), calls=%async_computation.5 | async-start | bytes 8388608 | tf_op jit(solution)/shard_map/all_to_all | solution.py:113
  167.1 240.9 %all-gather.5.cloned.1.call-start = ((), (), s32[]{:S(2)}) async-start(), calls=%async_computation.9 | async-start | bytes 5242880 | tf_op jit(solution)/shard_map/all_gather | solution.py:140
  168.9 2.4 copy-start.9
  168.9 2.5 copy-start.15
  171.3 1.6 copy-start.2
  171.9 1.0 copy-start.3
  259.6 114.0 %all-to-all-start.3 = ((f32[64,64,256]{2,1,0:T(8,128)}), f32[64,64,256]{2,1,0:T(8,128)}, u32[]{:S(2)}, u32[]{:S(2)}) async-start(f32[64,64,256]{2,1,0:T(8,128)} %scatter_fusion), calls=%async_computation.3 | async-start | bytes 8388608 | tf_op jit(solution)/shard_map/all_to_all | solution.py:112
  264.2 152.4 %reduce-scatter.2.cloned.1.call-start = ((), (), s32[]{:S(2)}) async-start(), calls=%async_computation.10 | async-start | bytes 2359296 | tf_op jit(solution)/shard_map/reduce_scatter | solution.py:136
  373.6 13.7 %all-to-all-start.6 = ((bf16[4,320,256]{2,1,0:T(8,128)(2,1)}), bf16[4,320,256]{2,1,0:T(8,128)(2,1)S(1)}, u32[]{:S(2)}, u32[]{:S(2)}) async-start(bf16[4,320,256]{2,1,0:T(8,128)(2,1)} %all_to_all.56), calls=%async_computation.6 | async-start | bytes 1310720 | tf_op jit(solution)/shard_map/all_to_all | solution.py:144
  387.3 4.4 %copy-start.6 = (bf16[4,320,256]{2,1,0:T(8,128)(2,1)}, bf16[4,320,256]{2,1,0:T(8,128)(2,1)S(1)}, u32[]{:S(2)}) copy-start(bf16[4,320,256]{2,1,0:T(8,128)(2,1)S(1)} %all-to-all-done.6) | copy-start | bytes 1966084
  387.3 14.7 %all-to-all-start.4 = ((bf16[4,320,256]{2,1,0:T(8,128)(2,1)}), bf16[4,320,256]{2,1,0:T(8,128)(2,1)}, u32[]{:S(2)}, u32[]{:S(2)}) async-start(bf16[4,320,256]{2,1,0:T(8,128)(2,1)} %all_to_all.51), calls=%async_computation.4 | async-start | bytes 1310720 | tf_op jit(solution)/shard_map/all_to_all | solution.py:143
  391.7 8.1 %copy-start.4 = (bf16[8,2,128,256]{2,3,1,0:T(8,128)(2,1)S(1)}, bf16[8,2,128,256]{2,3,1,0:T(8,128)(2,1)}, u32[]{:S(2)}) copy-start(bf16[8,2,128,256]{2,3,1,0:T(8,128)(2,1)} %copy-done.3) | copy-start | bytes 3145732
  400.2 1.7 copy-start.7
Sparse Core Ops, SparseCore 0:
  94.6 36.2 all-gather.2
  169.5 36.2 all-gather.4
Sparse Core Ops, SparseCore 1:
  276.7 120.6 reduce-scatter.1
where the time goes:
time: 425 us; the launch traced here: 424 us
  waiting for transfers between devices  214 us (50%)
  local copies, waits for them, and re-layouts  60.5 us (14%)
  blocking collectives  53.7 us (13%)
  starting transfers between devices  29.2 us (7%)
  matrix products  27.1 us (6%)
  other arithmetic  23.3 us (5%)
  between operations  15.9 us (4%)
    all_to_all x1, waiting for transfers between devices, local(): lax.all_to_all(outgoing_keys, 'st', split_axis=0, concat_axis=0, tiled=True)  95.6 us
    all_to_all x1, waiting for transfers between devices, local(): lax.all_to_all(outgoing_values, 'st', split_axis=0, concat_axis=0, tiled=...  72.3 us
    all_to_all x1, blocking collectives, local(): lax.all_to_all(picked_keys, 'st', split_axis=0, concat_axis=0, tiled=True)  53.7 us
    all_to_all x1, waiting for transfers between devices, local(): lax.all_to_all(picked_values, 'st', split_axis=0, concat_axis=0, tiled=True)  42.4 us
    unnamed x42, local copies, waits for them, and re-layouts  15.1 us
    dot_general x2, matrix products, contract(): lax.dot_general(left, right, (((1,), (1,)), ((), ())), preferred_element_...  8.81 us
  transfers between devices with their start and end apart: 9, of which 4 were waited for; matrix products, arithmetic and copies ran while one was open for 23% of the time, Pallas kernels for 0%

commit v1 on v0

--- a/solution.py
+++ b/solution.py
@@ -1,6 +1,10 @@
+import functools
+
 import jax
 import jax.numpy as jnp
 from jax import lax
+from jax.experimental import pallas as pl
+from jax.experimental.pallas import tpu as pltpu
 from jax.sharding import PartitionSpec as P
 
 HD = 128
@@ -20,7 +24,7 @@
     )
 
 
-def local(queries, gate_pre, cotangent, store, store_gain, w_key, w_value, owners, slots):
+def passage_plan(queries, gate_pre, cotangent, store, store_gain, w_key, w_value, owners, slots):
     st_size = lax.axis_size("st")
     tp_size = lax.axis_size("tp")
     blocks, per_block = owners.shape
@@ -105,27 +109,25 @@
     )
     grad_keys = grad_keys.reshape(slot_count, passage_len, local_width)
     grad_values = grad_values.reshape(slot_count, passage_len, local_width)
-    empty_slots = jnp.zeros((st_size * slot_cap, passage_len, local_width), jnp.float32)
-    outgoing_keys = empty_slots.at[position].set(grad_keys)
-    outgoing_values = empty_slots.at[position].set(grad_values)
+    empty_slots = jnp.zeros((st_size * slot_cap, passage_len, local_width), jnp.bfloat16)
+    outgoing_keys = empty_slots.at[position].set(grad_keys.astype(jnp.bfloat16))
+    outgoing_values = empty_slots.at[position].set(grad_values.astype(jnp.bfloat16))
     back_keys, back_values = (
         lax.all_to_all(outgoing_keys, "st", split_axis=0, concat_axis=0, tiled=True),
         lax.all_to_all(outgoing_values, "st", split_axis=0, concat_axis=0, tiled=True),
     )
     asked_flat = asked_ids.reshape(-1)
     owner_pick = (asked_flat[None, :] == jnp.arange(passages, dtype=jnp.int32)[:, None]).astype(
-        jnp.float32
+        jnp.bfloat16
     )
     passage_keys = jnp.dot(
         owner_pick,
         back_keys.reshape(st_size * slot_cap, passage_len * local_width),
-        precision=lax.Precision.HIGHEST,
         preferred_element_type=jnp.float32,
     )
     passage_values = jnp.dot(
         owner_pick,
         back_values.reshape(st_size * slot_cap, passage_len * local_width),
-        precision=lax.Precision.HIGHEST,
         preferred_element_type=jnp.float32,
     )
     passage_keys = passage_keys.astype(jnp.bfloat16).reshape(rows_dev, local_width)
@@ -153,6 +155,343 @@
         grad_unit - unit_rows * jnp.mean(grad_unit * unit_rows, axis=-1, keepdims=True)
     )
     return (grad_queries, grad_store, grad_w_value)
+
+
+FAR = -1e30
+MESH = pl.DeviceIdType.MESH
+
+
+def place_of(index, n):
+    odd = index % 2
+    return (1 - odd) * (index // 2) + odd * (n - 1 - index // 2)
+
+
+def index_at(place, n):
+    place = (place + 2 * n) % n
+    back = place // (n // 2)
+    return (1 - back) * (2 * place) + back * (2 * (n - 1 - place) + 1)
+
+
+def greet(right, left):
+    barrier = pltpu.get_barrier_semaphore()
+    for neighbour in (left, right):
+        pl.semaphore_signal(barrier, inc=1, device_id={"st": neighbour}, device_id_type=MESH)
+    pl.semaphore_wait(barrier, 2)
+
+
+def gather_kernel(n, q_ref, g_ref, q_all, g_all, send_sem, recv_sem, own_sem):
+    me = lax.axis_index("st")
+    place = place_of(me, n)
+    right, left = index_at(place + 1, n), index_at(place - 1, n)
+    half_rows = q_ref.shape[0] // 2
+    greet(right, left)
+    own = []
+    for number, (src, dst) in enumerate(((q_ref, q_all), (g_ref, g_all))):
+        copy = pltpu.make_async_copy(src, dst.at[me], own_sem.at[number])
+        copy.start()
+        own.append(copy)
+    hops = n // 2
+
+    def piece(side, step, part):
+        number, half = part // 2, part % 2
+        src, dst = ((q_ref, q_all), (g_ref, g_all))[number]
+        origin = index_at(place - step, n) if side == 0 else index_at(place + step, n)
+        rows = pl.ds(half * half_rows, half_rows)
+        return pltpu.make_async_remote_copy(
+            src_ref=src.at[rows] if step == 0 else dst.at[origin, rows],
+            dst_ref=dst.at[origin, rows],
+            send_sem=send_sem.at[side, step, part],
+            recv_sem=recv_sem.at[side, step, part],
+            device_id={"st": right if side == 0 else left},
+            device_id_type=MESH,
+        )
+
+    started = []
+    for step in range(hops):
+        for part in range(4):
+            for side in range(2):
+                if step > 0 and (step < hops - 1 or part % 2 == side):
+                    piece(side, step - 1, part).wait_recv()
+                if step < hops - 1 or part % 2 == side:
+                    copy = piece(side, step, part)
+                    copy.start()
+                    started.append(copy)
+    for part in range(4):
+        for side in range(2):
+            if part % 2 != side:
+                piece(side, hops - 2, part).wait_recv()
+    for part in range(4):
+        piece(part % 2, hops - 1, part).wait_recv()
+    for copy in own:
+        copy.wait()
+    for copy in started:
+        copy.wait_send()
+
+
+def ring_gather(queries, grad_in, n):
+    rows, width = queries.shape
+    hops = n // 2
+    shape = jax.ShapeDtypeStruct((n, rows, width), jnp.bfloat16)
+    vmem = pl.BlockSpec(memory_space=pltpu.VMEM)
+    return pl.pallas_call(
+        functools.partial(gather_kernel, n),
+        out_shape=(shape, shape),
+        in_specs=[vmem, vmem],
+        out_specs=(vmem, vmem),
+        scratch_shapes=[
+            pltpu.SemaphoreType.DMA((2, hops, 4)),
+            pltpu.SemaphoreType.DMA((2, hops, 4)),
+            pltpu.SemaphoreType.DMA((2,)),
+        ],
+        compiler_params=pltpu.CompilerParams(collective_id=0, has_side_effects=True, vmem_limit_bytes=40 << 20),
+        name="ring_gather",
+    )(queries, grad_in)
+
+
+def scatter_kernel(n, parts, x_ref, out_ref, send_buf, recv_buf, send_sem, recv_sem):
+    me = lax.axis_index("st")
+    place = place_of(me, n)
+    right, left = index_at(place + 1, n), index_at(place - 1, n)
+    rows = x_ref.shape[1]
+    span = rows // parts
+    greet(right, left)
+    hops = n // 2
+
+    def used(side, step, part):
+        return step > 0 or (part < parts // 2) == (side == 0)
+
+    def piece(side, step, part):
+        return pltpu.make_async_remote_copy(
+            src_ref=send_buf.at[side, step, pl.ds(part * span, span)],
+            dst_ref=recv_buf.at[side, step, pl.ds(part * span, span)],
+            send_sem=send_sem.at[side, step, part],
+            recv_sem=recv_sem.at[side, step, part],
+            device_id={"st": right if side == 0 else left},
+            device_id_type=MESH,
+        )
+
+    started = []
+    for step in range(hops):
+        for part in range(parts):
+            for side in range(2):
+                if not used(side, step, part):
+                    continue
+                distance = hops - step
+                dest = index_at(place + distance, n) if side == 0 else index_at(place - distance, n)
+                at = pl.ds(part * span, span)
+                total = x_ref[dest, at]
+                if step > 0 and used(side, step - 1, part):
+                    piece(side, step - 1, part).wait_recv()
+                    total = (total.astype(jnp.float32) + recv_buf[side, step - 1, at].astype(jnp.float32)).astype(jnp.bfloat16)
+                send_buf[side, step, at] = total
+                copy = piece(side, step, part)
+                copy.start()
+                started.append(copy)
+    for part in range(parts):
+        at = pl.ds(part * span, span)
+        total = x_ref[me, at].astype(jnp.float32)
+        for side in range(2):
+            piece(side, hops - 1, part).wait_recv()
+            total = total + recv_buf[side, hops - 1, at].astype(jnp.float32)
+        out_ref[at] = total
+    for copy in started:
+        copy.wait_send()
+
+
+def ring_scatter(terms, n):
+    rows, width = terms.shape[1:]
+    hops = n // 2
+    parts = 4
+    vmem = pl.BlockSpec(memory_space=pltpu.VMEM)
+    return pl.pallas_call(
+        functools.partial(scatter_kernel, n, parts),
+        out_shape=jax.ShapeDtypeStruct((rows, width), jnp.float32),
+        in_specs=[vmem],
+        out_specs=vmem,
+        scratch_shapes=[
+            pltpu.VMEM((2, hops, rows, width), jnp.bfloat16),
+            pltpu.VMEM((2, hops, rows, width), jnp.bfloat16),
+            pltpu.SemaphoreType.DMA((2, hops, parts)),
+            pltpu.SemaphoreType.DMA((2, hops, parts)),
+        ],
+        compiler_params=pltpu.CompilerParams(collective_id=1, has_side_effects=True, vmem_limit_bytes=40 << 20),
+        name="ring_scatter",
+    )(terms)
+
+
+NT = (((1,), (1,)), ((), ()))
+TN = (((0,), (0,)), ((), ()))
+
+
+def dot(left, right, dims=(((1,), (0,)), ((), ()))):
+    return lax.dot_general(left, right, dims, preferred_element_type=jnp.float32)
+
+
+def stats_kernel(blocks, heads, ids, q_ref, g_ref, k_ref, v_ref, out_ref):
+    scale = HD ** (-0.5)
+    block_len = q_ref.shape[1] // blocks
+
+    @pl.loop(0, blocks)
+    def _(block):
+        picked = ids[pl.program_id(0) * blocks + block]
+
+        @pl.when(picked < 0)
+        def _():
+            for head in range(heads):
+                out_ref[block, 2 * head] = jnp.full((block_len,), FAR, jnp.float32)
+                out_ref[block, 2 * head + 1] = jnp.zeros((block_len,), jnp.float32)
+
+        @pl.when(picked >= 0)
+        def _():
+            tokens = pl.ds(pl.multiple_of(block * block_len, block_len), block_len)
+            for head in range(heads):
+                cols = pl.ds(head * HD, HD)
+                scores = dot(k_ref[picked, :, cols], q_ref[0, tokens, cols], NT) * scale
+                grads = dot(v_ref[picked, :, cols], g_ref[0, tokens, cols], NT)
+                top = jnp.max(scores, axis=0, keepdims=True)
+                raised = jnp.exp(scores - top)
+                total = jnp.sum(raised, axis=0, keepdims=True)
+                mean = jnp.sum(raised * grads, axis=0, keepdims=True) / total
+                out_ref[block, pl.ds(2 * head, 1)] = top + jnp.log(total)
+                out_ref[block, pl.ds(2 * head + 1, 1)] = mean
+
+
+def grads_kernel(blocks, heads, ids, q_ref, g_ref, k_ref, v_ref, s_ref, dq_ref, pk_ref, pv_ref, dk_acc, dv_acc):
+    scale = HD ** (-0.5)
+    block_len = q_ref.shape[1] // blocks
+
+    @pl.when(pl.program_id(0) == 0)
+    def _():
+        dk_acc[...] = jnp.zeros_like(dk_acc)
+        dv_acc[...] = jnp.zeros_like(dv_acc)
+
+    @pl.loop(0, blocks)
+    def _(block):
+        picked = ids[pl.program_id(0) * blocks + block]
+        tokens = pl.ds(pl.multiple_of(block * block_len, block_len), block_len)
+
+        @pl.when(picked < 0)
+        def _():
+            dq_ref[0, tokens] = jnp.zeros((block_len, heads * HD), jnp.bfloat16)
+
+        @pl.when(picked >= 0)
+        def _():
+            for head in range(heads):
+                cols = pl.ds(head * HD, HD)
+                keys = k_ref[picked, :, cols]
+                tok_q, tok_g = q_ref[0, tokens, cols], g_ref[0, tokens, cols]
+                scores = dot(keys, tok_q, NT) * scale
+                grads = dot(v_ref[picked, :, cols], tok_g, NT)
+                weights = jnp.exp(scores - s_ref[block, pl.ds(2 * head, 1)])
+                half = (weights * (grads - s_ref[block, pl.ds(2 * head + 1, 1)])).astype(jnp.bfloat16)
+                dq_ref[0, tokens, cols] = (dot(half, keys, TN) * scale).astype(jnp.bfloat16)
+                dk_acc[picked, :, cols] += dot(half, tok_q) * scale
+                dv_acc[picked, :, cols] += dot(weights.astype(jnp.bfloat16), tok_g)
+
+    @pl.when(pl.program_id(0) == pl.num_programs(0) - 1)
+    def _():
+        pk_ref[...] = dk_acc[...].astype(jnp.bfloat16)
+        pv_ref[...] = dv_acc[...].astype(jnp.bfloat16)
+
+
+def query_plan(queries, gate_pre, cotangent, store, store_gain, w_key, w_value, owners, slots):
+    n = lax.axis_size("st")
+    tp_size = lax.axis_size("tp")
+    me = lax.axis_index("st")
+    blocks, per_block = owners.shape
+    tok_rows, local_width = queries.shape
+    heads = local_width // HD
+    block_len = tok_rows // blocks
+    rows_dev = store.shape[0]
+    passages = rows_dev // PLEN
+    named = owners * passages + slots
+    all_named = lax.all_gather(named, "st", axis=0, tiled=True)
+    held = all_named - me * passages
+    ids = jnp.max(jnp.where((held >= 0) & (held < passages), held, -1), axis=1)
+    gate_open = jax.nn.sigmoid(gate_pre.astype(jnp.float32))
+    grad_in = (gate_open * cotangent.astype(jnp.float32)).astype(jnp.bfloat16)
+    q_all, g_all = ring_gather(queries, grad_in, n)
+    store_rows = store.astype(jnp.float32)
+    row_inverse = row_scale(store_rows)
+    normed = (store_rows * row_inverse * store_gain).astype(jnp.bfloat16)
+    key_table = jnp.dot(normed, w_key, preferred_element_type=jnp.float32).astype(jnp.bfloat16)
+    value_table = jnp.dot(normed, w_value, preferred_element_type=jnp.float32).astype(jnp.bfloat16)
+    key_table = key_table.reshape(passages, PLEN, local_width)
+    value_table = value_table.reshape(passages, PLEN, local_width)
+    token_spec = pl.BlockSpec((1, tok_rows, local_width), lambda i, ids: (i, 0, 0))
+    table_spec = pl.BlockSpec((passages, PLEN, local_width), lambda i, ids: (0, 0, 0))
+    stat_spec = pl.BlockSpec((blocks, 2 * heads, block_len), lambda i, ids: (i, 0, 0))
+    stats = pl.pallas_call(
+        functools.partial(stats_kernel, blocks, heads),
+        out_shape=jax.ShapeDtypeStruct((n * blocks, 2 * heads, block_len), jnp.float32),
+        grid_spec=pltpu.PrefetchScalarGridSpec(
+            num_scalar_prefetch=1,
+            grid=(n,),
+            in_specs=[token_spec, token_spec, table_spec, table_spec],
+            out_specs=stat_spec,
+        ),
+        name="stats",
+    )(ids, q_all, g_all, key_table, value_table)
+    every = lax.all_gather(stats, "st", axis=0)
+    every = every.reshape(n, n * blocks, heads, 2, block_len)
+    logs, means = every[:, :, :, 0], every[:, :, :, 1]
+    top = jnp.max(logs, axis=0)
+    shares = jnp.exp(logs - top)
+    total = jnp.sum(shares, axis=0)
+    log_all = top + jnp.log(total)
+    delta = jnp.sum(shares * means, axis=0) / total
+    joined = jnp.stack([log_all, delta], axis=2).reshape(n * blocks, 2 * heads, block_len)
+    dq, passage_keys, passage_values = pl.pallas_call(
+        functools.partial(grads_kernel, blocks, heads),
+        out_shape=(
+            jax.ShapeDtypeStruct((n, tok_rows, local_width), jnp.bfloat16),
+            jax.ShapeDtypeStruct((passages, PLEN, local_width), jnp.bfloat16),
+            jax.ShapeDtypeStruct((passages, PLEN, local_width), jnp.bfloat16),
+        ),
+        grid_spec=pltpu.PrefetchScalarGridSpec(
+            num_scalar_prefetch=1,
+            grid=(n,),
+            in_specs=[token_spec, token_spec, table_spec, table_spec, stat_spec],
+            out_specs=(token_spec, table_spec, table_spec),
+            scratch_shapes=[pltpu.VMEM((passages, PLEN, local_width), jnp.float32)] * 2,
+        ),
+        name="grads",
+    )(ids, q_all, g_all, key_table, value_table, joined)
+    passage_keys = passage_keys.reshape(rows_dev, local_width)
+    passage_values = passage_values.reshape(rows_dev, local_width)
+    weight_terms = lax.dot_general(
+        normed, passage_values, (((0,), (0,)), ((), ())), preferred_element_type=jnp.float32
+    )
+    grad_w_value = lax.psum_scatter(weight_terms, "st", scatter_dimension=0, tiled=True)
+    grad_queries = ring_scatter(dq, n)
+    quarter = rows_dev // tp_size
+    whole_key, whole_value = (
+        lax.all_gather(w_key, "tp", axis=1, tiled=True),
+        lax.all_gather(w_value, "tp", axis=1, tiled=True),
+    )
+    own_keys, own_values = (
+        lax.all_to_all(passage_keys, "tp", split_axis=0, concat_axis=1, tiled=True),
+        lax.all_to_all(passage_values, "tp", split_axis=0, concat_axis=1, tiled=True),
+    )
+    grad_normed = contract(own_keys, whole_key) + contract(own_values, whole_value)
+    first_row = lax.axis_index("tp") * quarter
+    own_rows = lax.dynamic_slice_in_dim(store, first_row, quarter, 0).astype(jnp.float32)
+    own_inverse = row_scale(own_rows)
+    unit_rows = own_rows * own_inverse
+    grad_unit = grad_normed * store_gain
+    grad_store = own_inverse * (
+        grad_unit - unit_rows * jnp.mean(grad_unit * unit_rows, axis=-1, keepdims=True)
+    )
+    return (grad_queries, grad_store, grad_w_value)
+
+
+def local(*arrays):
+    queries, owners = arrays[0], arrays[7]
+    n = lax.axis_size("st")
+    slot_cap = (2 * owners.size + n - 1) // n
+    if n % 2 == 0 and n >= 4 and 8 * slot_cap * PLEN >= 3 * queries.shape[0]:
+        return query_plan(*arrays)
+    return passage_plan(*arrays)
 
 
 def solution(mesh):

time: 425 us -> 362 us (0.85)
  Pallas kernels: 0 us -> 190 us
  waiting for transfers between devices: 214 us -> 69.6 us
  local copies, waits for them, and re-layouts: 60.5 us -> 10.2 us
  starting transfers between devices: 29.2 us -> 3.82 us
  blocking collectives: 53.7 us -> 40.7 us
  other arithmetic: 23.3 us -> 11.3 us
    all_to_all x6 -> x1, waiting for transfers between devices: 213 us -> 0.01 us  [query_plan(): lax.all_to_all(passage_values, 'tp', split_axis=0, concat_axis=1, tiled=T...]
    pallas_call x0 -> x4, Pallas kernels: none -> 190 us  [the longest x1 77.3 us: ring_gather(): pl.pallas_call(functools.partial(gather_kernel, n), out_shape=(shape, sha...]
    all_gather x2 -> x3, waiting for transfers between devices: 0.02 us -> 44.9 us  [the longest x1 44.9 us: query_plan(): every = lax.all_gather(stats, 'st', axis=0)]
    all_to_all x1, blocking collectives: 53.7 us -> 12.7 us  [query_plan(): lax.all_to_all(passage_keys, 'tp', split_axis=0, concat_axis=1, tiled=True)]
    all_gather x0 -> x1, blocking collectives: none -> 27.9 us  [query_plan(): all_named = lax.all_gather(named, 'st', axis=0, tiled=True)]
    all_to_all x6 -> x1, starting transfers between devices: 28.9 us -> 3.67 us  [query_plan(): lax.all_to_all(passage_values, 'tp', split_axis=0, concat_axis=1, tiled=T...]
    reduce_scatter x1, waiting for transfers between devices: 0.01 us -> 23.3 us  [query_plan(): lax.psum_scatter(weight_terms, 'st', scatter_dimension=0, tiled=True)]
    reshape x12 -> x0, local copies, waits for them, and re-layouts: 10.9 us -> none  [the longest x1 3.03 us: local(): grad_keys = grad_keys.reshape(slot_count, passage_len, local_width)]
  transfers between devices with their start and end apart: 9 -> 5, of which waited for: 4 -> 2; matrix products, arithmetic and copies ran while one was open for 23% -> 7% of each run, Pallas kernels for 0% -> 28%
where the time goes in v1:
time: 362 us; the launch traced here: 363 us
  Pallas kernels  190 us (52%)
  waiting for transfers between devices  69.6 us (19%)
  blocking collectives  40.7 us (11%)
  matrix products  23.1 us (6%)
  between operations  14 us (4%)
  other arithmetic  11.3 us (3%)
  local copies, waits for them, and re-layouts  10.2 us (3%)
  starting transfers between devices  3.82 us (1%)
    pallas_call x1, Pallas kernels, ring_gather(): pl.pallas_call(functools.partial(gather_kernel, n), out_shape=(shape, sha...  77.3 us
    pallas_call x1, Pallas kernels, ring_scatter(): pl.pallas_call(functools.partial(scatter_kernel, n, parts), out_shape=jax...  73.8 us
    all_gather x1, waiting for transfers between devices, query_plan(): every = lax.all_gather(stats, 'st', axis=0)  44.9 us
    all_gather x1, blocking collectives, query_plan(): all_named = lax.all_gather(named, 'st', axis=0, tiled=True)  27.9 us
    pallas_call x1, Pallas kernels, query_plan(): pl.pallas_call(functools.partial(grads_kernel, blocks, heads), out_shape=...  26.6 us
    reduce_scatter x1, waiting for transfers between devices, query_plan(): lax.psum_scatter(weight_terms, 'st', scatter_dimension=0, tiled=True)  23.3 us
    all_to_all x1, blocking collectives, query_plan(): lax.all_to_all(passage_keys, 'tp', split_axis=0, concat_axis=1, tiled=True)  12.7 us
    pallas_call x1, Pallas kernels, query_plan(): pl.pallas_call(functools.partial(stats_kernel, blocks, heads), out_shape=...  12.6 us
  transfers between devices with their start and end apart: 5, of which 2 were waited for; matrix products, arithmetic and copies ran while one was open for 7% of the time, Pallas kernels for 28%

profile of v1, /device:TPU:0, one launch (start us, length us, event | category | flops | bytes accessed | tf_op | source)
XLA Modules:
  0.0 363.0 jit_solution(18076401751621638387)
XLA Ops:
  7.2 0.0 copy-start.11
  7.2 0.0 all-gather.10.cloned.1.call-start
  7.2 0.0 copy-start.4
  7.2 3.7 %fusion = f32[1280]{0:T(1024)S(1)} fusion(bf16[1280,2048]{1,0:T(8,128)(2,1)} %param.12), kind=kLoop, calls=%fused_computation.2 | loop fusion | flops 7863040 | bytes 5248000 | tf_op jit(solution)/shard_map/reduce_sum | solution.py:18
  11.0 0.0 copy-done.11
  11.0 0.3 copy-done.4
  11.3 3.8 %convolution_convert_fusion.1 = bf16[1280,256]{1,0:T(8,128)(2,1)} fusion(bf16[2048,256]{1,0:T(8,128)(2,1)} %param.14, bf16[1280,2048]{1,0:T(8,128)(2,1)S(1)} %copy-done.4, f32[2048]{0:T(1024)S(1)} %copy-done.11, f32[1280]{0:T(1024)S(1)} %add_rsqrt_fusion), kind=kOutput, calls=%fused_computation.16 | convolution fusion | flops 1352990720 | bytes 6960128 | tf_op jit(solution)/shard_map/dot_general | solution.py:417
  15.1 0.0 copy-start.8
  15.1 0.0 copy-start.3
  15.2 2.6 convolution_convert_fusion
  17.7 27.9 %all-gather.1 = s32[8,8,4]{1,2,0:T(4,128)S(1)} all-gather(s32[1,8,4]{1,2,0:T(4,128)S(1)} %add_bitcast_fusion), channel_id=1, replica_groups=mesh['st'=8,'tp'=4] {'st'}, dimensions={0}, use_global_device_ids=true | all-gather | bytes 1152 | tf_op jit(solution)/shard_map/all_gather | solution.py:408
  45.7 0.1 reshape.90
  45.8 0.6 select_reduce_fusion.ids
  46.4 0.0 copy-done.7
  46.4 0.3 multiply_convert_fusion.g_ref
  46.7 77.3 %ring_gather.1 = (bf16[8,1024,256]{2,1,0:T(8,128)(2,1)S(1)}, bf16[8,1024,256]{2,1,0:T(8,128)(2,1)S(1)}) custom-call(bf16[1024,256]{1,0:T(8,128)(2,1)S(1)} %copy-done.3, bf16[1024,256]{1,0:T(8,128)(2,1)S(1)} %multiply_convert_fusion.g_ref), custom_call_target="tpu_custom_call" | custom-call | tf_op jit(solution)/shard_map/ring_gather/pallas_call | solution.py:236
  123.9 0.0 copy-start
  124.0 1.9 copy-done
  125.9 1.9 copy-done.1
  127.8 12.6 %stats.1 = f32[64,4,128]{2,1,0:T(4,128)} custom-call(s32[64]{0:T(128)} %select_reduce_fusion.ids, bf16[8,1024,256]{2,1,0:T(8,128)(2,1)} %copy-done, bf16[8,1024,256]{2,1,0:T(8,128)(2,1)} %copy-done.1, bf16[20,64,256]{2,1,0:T(8,128)(2,1)} %bitcast.39, bf16[20,64,256]{2,1,0:T(8,128)(2,1)} %bitcast.41), custom_call_target="tpu_custom_call" | custom-call | tf_op jit(solution)/shard_map/stats/pallas_call | solution.py:424
  140.4 0.0 all-gather.10.cloned.1.call-update
  140.5 0.0 all-gather.6.cloned.1.call-start
  140.5 0.7 all-gather.6.cloned.1.call-update
  141.2 0.0 all-gather.8.cloned.1.call-start
  141.3 0.7 all-gather.8.cloned.1.call-update
  142.0 0.0 reduce-scatter.2.cloned.1.call-start
  142.0 44.9 %all-gather.10.cloned.1.call-done = f32[512,4,128]{2,1,0:T(4,128)} async-done(((f32[64,4,128]{2,1,0:T(4,128)}), f32[512,4,128]{2,1,0:T(4,128)}) %all-gather.10.cloned.1.call-update) | async-done | bytes 1048592 | tf_op jit(solution)/shard_map/all_gather | solution.py:435
  186.9 2.6 fusion.15
  189.5 0.2 reduce_max.19
  189.8 0.6 fusion.10
  190.4 0.8 pad_maximum_fusion
  191.2 26.6 %grads.1 = (bf16[8,1024,256]{2,1,0:T(8,128)(2,1)}, bf16[20,64,256]{2,1,0:T(8,128)(2,1)}, bf16[20,64,256]{2,1,0:T(8,128)(2,1)}) custom-call(s32[64]{0:T(128)} %select_reduce_fusion.ids, bf16[8,1024,256]{2,1,0:T(8,128)(2,1)} %copy-done, bf16[8,1024,256]{2,1,0:T(8,128)(2,1)} %copy-done.1, bf16[20,64,256]{2,1,0:T(8,128)(2,1)} %bitcast.40, ...), custom_call_target="tpu_custom_call" | custom-call | tf_op jit(solution)/shard_map/grads/pallas_call | solution.py:444
  217.8 6.1 %fusion.11 = f32[2048,256]{1,0:T(8,128)} fusion(bf16[1280,256]{1,0:T(8,128)(2,1)} %bitcast.14, bf16[1280,2048]{1,0:T(8,128)(2,1)} %param.12, f32[2048]{0:T(1024)S(1)} %copy-done.11, f32[1280]{0:T(1024)S(1)} %add_rsqrt_fusion), kind=kOutput, calls=%fused_computation.29 | convolution fusion | flops 1352663040 | bytes 8008704 | tf_op jit(solution)/shard_map/dot_general | solution.py:462
  223.9 0.0 reduce-scatter.2.cloned.1.call-update
  223.9 12.7 %all_to_all.38 = bf16[4,320,256]{2,1,0:T(8,128)(2,1)S(1)} all-to-all(bf16[4,320,256]{2,1,0:T(8,128)(2,1)S(1)} %bitcast.47), channel_id=1, replica_groups=mesh['st'=8,'tp'=4] {'tp'}, dimensions={0} | all-to-all | bytes 1310720 | tf_op jit(solution)/shard_map/all_to_all | solution.py:473
  236.7 3.7 %all-to-all-start.1 = ((bf16[4,320,256]{2,1,0:T(8,128)(2,1)}), bf16[4,320,256]{2,1,0:T(8,128)(2,1)S(1)}, u32[]{:S(2)}, u32[]{:S(2)}) async-start(bf16[4,320,256]{2,1,0:T(8,128)(2,1)} %bitcast.12), calls=%async_computation.1 | async-start | bytes 1310720 | tf_op jit(solution)/shard_map/all_to_all | solution.py:474
  240.3 1.7 fusion.9
  242.0 2.2 copy-done.2
  244.2 73.8 %ring_scatter.1 = f32[1024,256]{1,0:T(8,128)S(1)} custom-call(bf16[8,1024,256]{2,1,0:T(8,128)(2,1)S(1)} %copy-done.2), custom_call_target="tpu_custom_call" | custom-call | tf_op jit(solution)/shard_map/ring_scatter/pallas_call | solution.py:306
  318.0 0.1 copy.30
  318.1 0.0 all-to-all-done.1
  318.1 0.1 copy.31
  318.2 0.0 all-gather.6.cloned.1.call-done
  318.2 5.3 %fusion.16 = f32[320,2048]{1,0:T(8,128)} fusion(bf16[320,1024]{1,0:T(8,128)(2,1)S(1)} %bitcast.49, bf16[2048,1024]{1,0:T(8,128)(2,1)} %all-gather.6.cloned.1.call-done), kind=kOutput, calls=%fused_computation.31 | convolution fusion | flops 1342177280 | bytes 7471104 | tf_op jit(solution)/shard_map/dot_general | solution.py:22
  323.6 5.3 %fusion.6 = (f32[320]{0:T(512)S(1)}, f32[320,2048]{1,0:T(8,128)S(1)}) fusion(f32[320]{0:T(512)S(1)} %add_rsqrt_fusion.1, bf16[1280,2048]{1,0:T(8,128)(2,1)} %param.12, s32[]{:T(128)S(6)} %select_n.8, f32[2048]{0:T(1024)S(1)} %copy-done.11, f32[320,2048]{1,0:T(8,128)} %fusion.16, bf16[320,1024]{1,0:T(8,128)(2,1)S(1)} %bitcast.48, ...), kind=kOutput, calls=%fused_computation.11 | convolution fusion | flops 1346109184 | bytes 11414020 | tf_op jit(solution)/shard_map/dot_general | solution.py:22
  328.9 3.3 fusion.8
  332.2 23.3 %reduce-scatter.2.cloned.1.call-done = f32[256,256]{1,0:T(8,128)} async-done(((f32[2048,256]{1,0:T(8,128)}), f32[256,256]{1,0:T(8,128)}) %reduce-scatter.2.cloned.1.call-update) | async-done | bytes 262160 | tf_op jit(solution)/shard_map/reduce_scatter | solution.py:465
  355.5 1.0 copy.34
  (20 shorter events, 0.1 us)
Async XLA Ops:
  7.2 3.8 %copy-start.11 = (f32[2048]{0:T(1024)S(1)}, f32[2048]{0:T(1024)}, u32[]{:S(2)}) copy-start(f32[2048]{0:T(1024)} %param.13) | copy-start | bytes 24580
  7.2 179.7 %all-gather.10.cloned.1.call-start = ((), (), s32[]{:S(2)}) async-start(), calls=%async_computation.6 | async-start | bytes 1179648 | tf_op jit(solution)/shard_map/all_gather | solution.py:435
  7.2 4.0 %copy-start.4 = (bf16[1280,2048]{1,0:T(8,128)(2,1)S(1)}, bf16[1280,2048]{1,0:T(8,128)(2,1)}, u32[]{:S(2)}) copy-start(bf16[1280,2048]{1,0:T(8,128)(2,1)} %param.12) | copy-start | bytes 15728644
  11.3 3.8 %copy-start.5 = (bf16[2048,256]{1,0:T(8,128)(2,1)S(1)}, bf16[2048,256]{1,0:T(8,128)(2,1)}, u32[]{:S(2)}) copy-start(bf16[2048,256]{1,0:T(8,128)(2,1)} %param.15) | copy-start | bytes 3145732
  15.1 2.6 copy-start.9
  15.1 2.6 copy-start.10
  15.1 31.2 %copy-start.7 = (bf16[1024,256]{1,0:T(8,128)(2,1)S(1)}, bf16[1024,256]{1,0:T(8,128)(2,1)}, u32[]{:S(2)}) copy-start(bf16[1024,256]{1,0:T(8,128)(2,1)} %param.11) | copy-start | bytes 1572868
  15.1 31.2 %copy-start.8 = (bf16[1024,256]{1,0:T(8,128)(2,1)S(1)}, bf16[1024,256]{1,0:T(8,128)(2,1)}, u32[]{:S(2)}) copy-start(bf16[1024,256]{1,0:T(8,128)(2,1)} %param.10) | copy-start | bytes 1572868
  15.1 31.5 %copy-start.3 = (bf16[1024,256]{1,0:T(8,128)(2,1)S(1)}, bf16[1024,256]{1,0:T(8,128)(2,1)}, u32[]{:S(2)}) copy-start(bf16[1024,256]{1,0:T(8,128)(2,1)} %q_ref.1) | copy-start | bytes 1572868
  123.9 2.0 copy-start
  125.9 1.9 copy-start.1
  140.5 177.8 %all-gather.6.cloned.1.call-start = ((), (), s32[]{:S(2)}) async-start(), calls=%async_computation.3 | async-start | bytes 5242880 | tf_op jit(solution)/shard_map/all_gather | solution.py:469
  141.2 182.3 %all-gather.8.cloned.1.call-start = ((), (), s32[]{:S(2)}) async-start(), calls=%async_computation.4 | async-start | bytes 5242880 | tf_op jit(solution)/shard_map/all_gather | solution.py:470
  142.0 213.5 %reduce-scatter.2.cloned.1.call-start = ((), (), s32[]{:S(2)}) async-start(), calls=%async_computation.5 | async-start | bytes 2359296 | tf_op jit(solution)/shard_map/reduce_scatter | solution.py:465
  217.8 6.1 %copy-start.6 = (bf16[20,64,256]{2,1,0:T(8,128)(2,1)S(1)}, bf16[20,64,256]{2,1,0:T(8,128)(2,1)}, u32[]{:S(2)}) copy-start(bf16[20,64,256]{2,1,0:T(8,128)(2,1)} %get-tuple-element.11) | copy-start | bytes 1966084
  236.7 81.5 %all-to-all-start.1 = ((bf16[4,320,256]{2,1,0:T(8,128)(2,1)}), bf16[4,320,256]{2,1,0:T(8,128)(2,1)S(1)}, u32[]{:S(2)}, u32[]{:S(2)}) async-start(bf16[4,320,256]{2,1,0:T(8,128)(2,1)} %bitcast.12), calls=%async_computation.1 | async-start | bytes 1310720 | tf_op jit(solution)/shard_map/all_to_all | solution.py:474
  242.0 2.2 copy-start.2
Sparse Core Ops, SparseCore 0:
  140.6 46.2 all-gather.9
  188.4 33.7 all-gather.5
  223.8 45.3 all-gather.7
  273.2 82.2 reduce-scatter.1
